TPU v7x, 32 devices: a whole 2x2x4 slice. The times are simulated.
32 devices in a mesh: sp: 8 (over z, y), tp: 4 (over x, core).
Axes of the slice: x: 2, y: 2, z: 4, core: 2. Of those that a mesh axis runs over, the one named last changes fastest.
Arguments:
- resid_in: bfloat16 [2048, 2048], P(('sp', 'tp')), may hold values from -6 to 6
- query_proj: bfloat16 [2048, 512], P('sp', 'tp'), may hold values from -6 to 6
- key_proj: bfloat16 [2048, 256], P('sp', 'tp'), may hold values from -6 to 6
- value_proj: bfloat16 [2048, 256], P('sp', 'tp'), may hold values from -6 to 6
- query_gain: float32 [8, 64], P('tp'), may hold values from 0.5 to 6
- key_gain: float32 [4, 64], P('tp'), may hold values from 0.5 to 6
- out_weight: bfloat16 [512, 2048], replicated, may hold values from -0.25 to 0.25
- norm_gain: float32 [2048], replicated, may hold values from 0.1 to 1.9
- gate_weight: bfloat16 [8, 2048, 1024], P('sp', None, 'tp'), may hold values from -0.125 to 0.125
- up_weight: bfloat16 [8, 2048, 1024], P('sp', None, 'tp'), may hold values from -0.125 to 0.125
- down_weight: bfloat16 [8, 1024, 2048], P('sp', 'tp'), may hold values from -0.1875 to 0.1875
- expert_ids: int32 [2048, 2], P('sp'), may hold values from 0 to 7, all different within a row; in each aligned block of 64 rows (0 to 63, 64 to 127, ...) at most 24 rows name the same one
- route_weight: float32 [2048, 2], P(('sp', 'tp')), may hold values from 0.2 to 1
Outputs:
- layer_out: bfloat16 [2048, 2048], P(('sp', 'tp'))
Inputs may be any that keep to these rules, and one draw needn't show every extreme that they name: `expert_ids`: each row names 2 different experts. In each aligned block of rows that one device holds (rows of one index of sp and tp together), no expert is named more than 24 times, and in some blocks one expert is named exactly 24 times.
All inputs are finite; a program needn't handle non-finite values.
Results may differ from a plain program's by a relative error of at most 0.014.
Values may be sent and summed in bfloat16 or wider, within the bound.
A program may use at most 64 MiB of HBM per device.

v0:
```python
import jax
import jax.numpy as jnp
from jax import lax
from jax.sharding import PartitionSpec as P

HEAD_DIM = 64
TOPK = 2
GRID_W = 64
TOK_DEV = 256


eps = 1e-06
rope_base = 10000.0


def rotary_tables(positions):
    row_pos = (positions // GRID_W).astype(jnp.float32)
    col_pos = (positions % GRID_W).astype(jnp.float32)
    freq_count = HEAD_DIM // 4
    inverse = rope_base ** (-jnp.arange(freq_count, dtype=jnp.float32) / freq_count)
    angles = jnp.concatenate([row_pos[:, None] * inverse, col_pos[:, None] * inverse], axis=-1)
    return (jnp.cos(angles), jnp.sin(angles))


def prepare(projected, gains, cosine, sine_table):
    tok_total = projected.shape[0]
    head_count = gains.shape[0]
    values_f = projected.astype(jnp.float32).reshape(tok_total, head_count, HEAD_DIM)
    normed = (
        values_f
        * lax.rsqrt(jnp.mean(values_f * values_f, axis=-1, keepdims=True) + eps)
        * gains[None]
    )
    half_dim = HEAD_DIM // 2
    first_half = normed[..., :half_dim]
    second_half = normed[..., half_dim:]
    cos_b = cosine[:, None, :]
    sin_b = sine_table[:, None, :]
    rotated = jnp.concatenate(
        [first_half * cos_b - second_half * sin_b, second_half * cos_b + first_half * sin_b],
        axis=-1,
    )
    return rotated.astype(jnp.bfloat16)


def slot_index(ids_rows, expert_count, capacity):
    flat_ids = ids_rows.reshape(-1)
    member = (flat_ids[:, None] == jnp.arange(expert_count, dtype=jnp.int32)[None, :]).astype(
        jnp.int32
    )
    ranks = jnp.sum((jnp.cumsum(member, axis=0) - member) * member, axis=1)
    return flat_ids * capacity + ranks


def build_send(rows, ids_rows, expert_count, capacity):
    slot_ids = slot_index(ids_rows, expert_count, capacity)
    picker = (
        jnp.arange(expert_count * capacity, dtype=jnp.int32)[:, None] == slot_ids[None, :]
    ).astype(jnp.bfloat16)
    repeated = jnp.repeat(rows, ids_rows.shape[1], axis=0)
    outgoing = jnp.dot(picker, repeated, preferred_element_type=jnp.float32).astype(jnp.bfloat16)
    return outgoing.reshape(expert_count, capacity, rows.shape[1])


def expert_ffn(rows, gate_local, up_local, down_local):
    lead_shape = rows.shape[:-1]
    flat_rows = rows.reshape(-1, rows.shape[-1])
    gate = jnp.dot(flat_rows, gate_local, preferred_element_type=jnp.float32)
    upper = jnp.dot(flat_rows, up_local, preferred_element_type=jnp.float32)
    hidden = (jax.nn.silu(gate) * upper).astype(jnp.bfloat16)
    result = jnp.dot(hidden, down_local, preferred_element_type=jnp.float32)
    return result.reshape(lead_shape + (down_local.shape[1],))


def body(
    resid_in,
    query_proj,
    key_proj,
    value_proj,
    query_gain,
    key_gain,
    out_weight,
    norm_gain,
    gate_weight,
    up_weight,
    down_weight,
    expert_ids,
    route_weight,
):
    tok_count = query_proj.shape[0]
    head_local = query_gain.shape[0]
    kv_local = key_gain.shape[0]
    group_size = head_local // kv_local
    positions = lax.axis_index("sp") * tok_count + lax.iota(jnp.int32, tok_count)
    cosine, sine_table = rotary_tables(positions)
    query_rot = prepare(query_proj, query_gain, cosine, sine_table)
    grouped = query_rot.reshape(tok_count, kv_local, group_size, HEAD_DIM)
    key_rot = prepare(key_proj, key_gain, cosine, sine_table).reshape(
        tok_count, kv_local * HEAD_DIM
    )
    score_factor = HEAD_DIM ** (-0.5)

    def attend_piece(running, segment):
        best_now, sums_now, accum_now = running
        seg_count = segment[0].shape[0]
        seg_keys = segment[0].reshape(seg_count, kv_local, HEAD_DIM)
        seg_values = segment[1].reshape(seg_count, kv_local, HEAD_DIM)
        scores = (
            jnp.einsum("qkgd,skd->qkgs", grouped, seg_keys, preferred_element_type=jnp.float32)
            * score_factor
        )
        new_best = jnp.maximum(best_now, jnp.max(scores, axis=-1))
        shrink = jnp.exp(best_now - new_best)
        exponents = jnp.exp(scores - new_best[..., None])
        sums_now = sums_now * shrink + jnp.sum(exponents, axis=-1)
        weights = exponents.astype(jnp.bfloat16)
        accum_now = accum_now * shrink[..., None] + jnp.einsum(
            "qkgs,skd->qkgd", weights, seg_values, preferred_element_type=jnp.float32
        )
        return (new_best, sums_now, accum_now)

    def attend_segment(running, segment):
        seg_count = segment[0].shape[0]
        if seg_count > 2048 and seg_count % 2048 == 0:
            sub_blocks = (
                segment[0].reshape(seg_count // 2048, 2048, segment[0].shape[1]),
                segment[1].reshape(seg_count // 2048, 2048, segment[1].shape[1]),
            )

            def scan_step(state_now, sub_block):
                return (attend_piece(state_now, sub_block), None)

            running, unused = lax.scan(scan_step, running, sub_blocks)
            return running
        return attend_piece(running, segment)

    initial = (
        jnp.full((tok_count, kv_local, group_size), -jnp.inf, jnp.float32),
        jnp.zeros((tok_count, kv_local, group_size), jnp.float32),
        jnp.zeros((tok_count, kv_local, group_size, HEAD_DIM), jnp.float32),
    )
    best_all, sums_all, accum_all = attend_segment(
        initial,
        (
            lax.all_gather(key_rot, "sp", axis=0, tiled=True),
            lax.all_gather(value_proj, "sp", axis=0, tiled=True),
        ),
    )
    attended = (
        (accum_all / sums_all[..., None])
        .astype(jnp.bfloat16)
        .reshape(tok_count, head_local * HEAD_DIM)
    )
    tp_count = lax.axis_size("tp")
    row_count = tok_count // tp_count
    regrouped = lax.all_to_all(attended, "tp", split_axis=0, concat_axis=1, tiled=True)
    mixed_out = jnp.dot(regrouped, out_weight, preferred_element_type=jnp.float32)
    residual = (resid_in.astype(jnp.float32) + mixed_out).astype(jnp.bfloat16)
    resid_f = residual.astype(jnp.float32)
    normed = (
        resid_f * lax.rsqrt(jnp.mean(resid_f * resid_f, axis=-1, keepdims=True) + eps) * norm_gain
    ).astype(jnp.bfloat16)
    expert_count = lax.axis_size("sp")
    capacity = max(2, 3 * TOPK * TOK_DEV // (2 * tp_count * expert_count))
    own_ids = lax.dynamic_slice_in_dim(expert_ids, lax.axis_index("tp") * row_count, row_count, 0)
    slot_ids = slot_index(own_ids, expert_count, capacity)
    gate_local = gate_weight[0]
    up_local = up_weight[0]
    down_local = down_weight[0]
    outgoing = build_send(normed, own_ids, expert_count, capacity)
    received = lax.all_to_all(outgoing, "sp", split_axis=0, concat_axis=0, tiled=True)
    partial_value = expert_ffn(
        lax.all_gather(received[None], "tp", axis=0, tiled=True), gate_local, up_local, down_local
    )
    summed = lax.psum_scatter(
        partial_value.astype(jnp.bfloat16), "tp", scatter_dimension=0, tiled=True
    ).astype(jnp.float32)
    expert_out = summed[0].astype(jnp.bfloat16)
    returned = lax.all_to_all(expert_out, "sp", split_axis=0, concat_axis=0, tiled=True)
    flat_out = returned.reshape(expert_count * capacity, returned.shape[-1])
    picked = (
        jnp.take(flat_out, slot_ids, axis=0)
        .astype(jnp.float32)
        .reshape(row_count, route_weight.shape[1], flat_out.shape[1])
    )
    combined = jnp.sum(picked * route_weight[:, :, None], axis=1)
    return (resid_f + combined).astype(jnp.bfloat16)


def solution(mesh):
    placed = (
        P(("sp", "tp"), None),
        P("sp", "tp"),
        P("sp", "tp"),
        P("sp", "tp"),
        P("tp", None),
        P("tp", None),
        P(),
        P(),
        P("sp", None, "tp"),
        P("sp", None, "tp"),
        P("sp", "tp", None),
        P("sp", None),
        P(("sp", "tp"), None),
    )
    return jax.shard_map(
        body, mesh=mesh, in_specs=placed, out_specs=P(("sp", "tp"), None), check_vma=False
    )
```

profile of v0, /device:TPU:0, one launch (start us, length us, event | category | flops | bytes accessed | tf_op | source)
XLA Modules:
  0.0 224.0 jit_solution(7668930817553734555)
XLA Ops:
  6.6 1.1 copy.30
  7.7 0.8 fusion.31
  8.5 0.8 fusion.33
  9.6 32.6 %all_gather.9 = bf16[2048,64]{0,1:T(8,128)(2,1)S(1)} all-gather(bf16[256,64]{0,1:T(8,128)(2,1)S(1)} %pad_maximum_fusion.1), channel_id=1, replica_groups=mesh['sp'=8,'tp'=4] {'sp'}, dimensions={0}, use_global_device_ids=true | all-gather | bytes 294912 | tf_op jit(solution)/shard_map/all_gather | solution.py:145
  42.2 0.8 multiply_multiply_fusion
  43.1 0.8 bitcast_reduce_fusion
  44.6 30.7 %all_gather.10 = bf16[2048,64]{0,1:T(8,128)(2,1)S(1)} all-gather(bf16[256,64]{0,1:T(8,128)(2,1)S(1)} %copy-done.3), channel_id=1, replica_groups=mesh['sp'=8,'tp'=4] {'sp'}, dimensions={0}, use_global_device_ids=true | all-gather | bytes 294912 | tf_op jit(solution)/shard_map/all_gather | solution.py:146
  75.3 0.8 fusion.21
  77.0 3.3 %all-to-all-start = ((bf16[4,64,128]{2,1,0:T(8,128)(2,1)}), bf16[4,64,128]{2,1,0:T(8,128)(2,1)S(1)}, u32[]{:S(2)}, u32[]{:S(2)}) async-start(bf16[4,64,128]{2,1,0:T(8,128)(2,1)} %copy.41), calls=%async_computation | async-start | bytes 131072 | tf_op jit(solution)/shard_map/all_to_all | solution.py:156
  81.1 3.2 %all-to-all-done = bf16[4,64,128]{2,1,0:T(8,128)(2,1)S(1)} async-done(((bf16[4,64,128]{2,1,0:T(8,128)(2,1)}), bf16[4,64,128]{2,1,0:T(8,128)(2,1)S(1)}, u32[]{:S(2)}, u32[]{:S(2)}) %all-to-all-start) | async-done | bytes 65568 | tf_op jit(solution)/shard_map/all_to_all | solution.py:156
  85.1 1.1 broadcast_in_dim.18
  86.2 1.2 reshape.371
  87.8 25.4 %all_to_all.29 = bf16[8,24,2048]{2,1,0:T(8,128)(2,1)} all-to-all(bf16[8,24,2048]{2,1,0:T(8,128)(2,1)S(1)} %bitcast.117), channel_id=1, replica_groups=mesh['sp'=8,'tp'=4] {'sp'}, dimensions={0} | all-to-all | bytes 1572864 | tf_op jit(solution)/shard_map/all_to_all | solution.py:171
  113.3 26.7 %all-gather.3.cloned.1.call-done = bf16[32,24,2048]{2,1,0:T(8,128)(2,1)} async-done(((bf16[8,24,2048]{2,1,0:T(8,128)(2,1)}), bf16[32,24,2048]{2,1,0:T(8,128)(2,1)}) %all-gather.3.cloned.1.call-update) | async-done | bytes 3145744 | tf_op jit(solution)/shard_map/all_gather | solution.py:173
  140.0 3.3 %fusion.26 = f32[768,256]{1,0:T(8,128)S(1)} fusion(bf16[768,2048]{1,0:T(8,128)(2,1)} %bitcast.121, bf16[1,2048,256]{2,1,0:T(8,128)(2,1)} %param.21), kind=kOutput, calls=%fused_computation.22 | convolution fusion | flops 805306368 | bytes 4980736 | tf_op jit(solution)/shard_map/dot_general | solution.py:68
  143.4 1.0 fusion.8
  144.7 2.6 %convolution_convert_fusion = bf16[4,8,24,2048]{3,2,1,0:T(8,128)(2,1)} fusion(bf16[4,8,24,256]{3,2,1,0:T(8,128)(2,1)S(1)} %bitcast.119, bf16[1,256,2048]{2,1,0:T(8,128)(2,1)S(1)} %copy-done.1), kind=kOutput, calls=%fused_computation.6 | convolution fusion | flops 806879232 | bytes 4587520 | tf_op jit(solution)/shard_map/dot_general | solution.py:71
  147.3 38.0 %reduce-scatter.2.cloned.1.call-done = bf16[1,8,24,2048]{3,2,1,0:T(8,128)(2,1)} async-done(((bf16[4,8,24,2048]{3,2,1,0:T(8,128)(2,1)}), bf16[1,8,24,2048]{3,2,1,0:T(8,128)(2,1)}) %reduce-scatter.2.cloned.1.call-update) | async-done | bytes 786448 | tf_op jit(solution)/shard_map/reduce_scatter | solution.py:175
  185.4 5.5 %all-to-all-start.2 = ((bf16[8,24,2048]{2,1,0:T(8,128)(2,1)}), bf16[8,24,2048]{2,1,0:T(8,128)(2,1)S(1)}, u32[]{:S(2)}, u32[]{:S(2)}) async-start(bf16[8,24,2048]{2,1,0:T(8,128)(2,1)} %bitcast.118), calls=%async_computation.3 | async-start | bytes 1572864 | tf_op jit(solution)/shard_map/all_to_all | solution.py:179
  191.6 19.4 %all-to-all-done.2 = bf16[8,24,2048]{2,1,0:T(8,128)(2,1)S(1)} async-done(((bf16[8,24,2048]{2,1,0:T(8,128)(2,1)}), bf16[8,24,2048]{2,1,0:T(8,128)(2,1)S(1)}, u32[]{:S(2)}, u32[]{:S(2)}) %all-to-all-start.2) | async-done | bytes 786464 | tf_op jit(solution)/shard_map/all_to_all | solution.py:179
  211.0 1.7 gather_fusion
  212.7 1.4 gather.7
  214.1 2.3 %multiply_reduce_fusion = f32[64,2048]{1,0:T(8,128)S(1)} fusion(bf16[64,2,2048]{2,1,0:T(2,128)(2,1)S(1)} %gather.7, pred[64,2]{1,0:T(8,128)(4,1)S(1)} %copy.36, f32[64,2]{1,0:T(8,128)S(1)} %copy.38), kind=kLoop, calls=%fused_computation.24 | loop fusion | flops 917504 | bytes 1049216 | tf_op jit(solution)/shard_map/reduce_sum | solution.py:186
  216.4 0.8 add_convert_fusion
  (56 shorter events, 5.0 us)
Async XLA Ops:
  6.5 77.8 %copy-start = (bf16[512,2048]{1,0:T(8,128)(2,1)S(1)}, bf16[512,2048]{1,0:T(8,128)(2,1)}, u32[]{:S(2)}) copy-start(bf16[512,2048]{1,0:T(8,128)(2,1)} %param.19) | copy-start | bytes 6291460
  43.0 1.5 copy-start.3
  43.8 36.5 %copy-start.6 = (s32[256,2]{0,1:T(2,128)S(1)}, s32[256,2]{0,1:T(2,128)}, u32[]{:S(2)}) copy-start(s32[256,2]{0,1:T(2,128)} %param.24) | copy-start | bytes 6148
  43.8 40.6 %copy-start.2 = (bf16[64,2048]{1,0:T(8,128)(2,1)S(1)}, bf16[64,2048]{1,0:T(8,128)(2,1)}, u32[]{:S(2)}) copy-start(bf16[64,2048]{1,0:T(8,128)(2,1)} %param.13) | copy-start | bytes 786436
  75.3 9.7 %copy-start.4 = (f32[2048]{0:T(1024)S(1)}, f32[2048]{0:T(1024)}, u32[]{:S(2)}) copy-start(f32[2048]{0:T(1024)} %param.20) | copy-start | bytes 24580
  77.0 7.4 %all-to-all-start = ((bf16[4,64,128]{2,1,0:T(8,128)(2,1)}), bf16[4,64,128]{2,1,0:T(8,128)(2,1)S(1)}, u32[]{:S(2)}, u32[]{:S(2)}) async-start(bf16[4,64,128]{2,1,0:T(8,128)(2,1)} %copy.41), calls=%async_computation | async-start | bytes 131072 | tf_op jit(solution)/shard_map/all_to_all | solution.py:156
  80.3 59.7 %all-gather.3.cloned.1.call-start = ((), (), s32[]{:S(2)}) async-start(), calls=%async_computation.5 | async-start | bytes 3932160 | tf_op jit(solution)/shard_map/all_gather | solution.py:173
  113.3 72.1 %reduce-scatter.2.cloned.1.call-start = ((), (), s32[]{:S(2)}) async-start(), calls=%async_computation.4 | async-start | bytes 3932160 | tf_op jit(solution)/shard_map/reduce_scatter | solution.py:175
  140.0 3.3 %copy-start.7 = (bf16[32,24,2048]{2,1,0:T(8,128)(2,1)S(1)}, bf16[32,24,2048]{2,1,0:T(8,128)(2,1)}, u32[]{:S(2)}) copy-start(bf16[32,24,2048]{2,1,0:T(8,128)(2,1)} %all-gather.3.cloned.1.call-done) | copy-start | bytes 9437188
  140.0 3.4 %copy-start.8 = (bf16[1,2048,256]{2,1,0:T(8,128)(2,1)S(1)}, bf16[1,2048,256]{2,1,0:T(8,128)(2,1)}, u32[]{:S(2)}) copy-start(bf16[1,2048,256]{2,1,0:T(8,128)(2,1)} %param.22) | copy-start | bytes 3145732
  143.4 1.2 copy-start.1
  144.7 46.8 %copy-start.5 = (f32[64,2]{0,1:T(2,128)S(1)}, f32[64,2]{0,1:T(2,128)}, u32[]{:S(2)}) copy-start(f32[64,2]{0,1:T(2,128)} %param.25) | copy-start | bytes 1540
  185.4 25.6 %all-to-all-start.2 = ((bf16[8,24,2048]{2,1,0:T(8,128)(2,1)}), bf16[8,24,2048]{2,1,0:T(8,128)(2,1)S(1)}, u32[]{:S(2)}, u32[]{:S(2)}) async-start(bf16[8,24,2048]{2,1,0:T(8,128)(2,1)} %bitcast.118), calls=%async_computation.3 | async-start | bytes 1572864 | tf_op jit(solution)/shard_map/all_to_all | solution.py:179
Sparse Core Ops, SparseCore 0:
  113.4 26.5 all-gather.2
  147.5 37.8 reduce-scatter.1
where the time goes:
time: 225 us; the launch traced here: 224 us
  blocking collectives  88.7 us (39%)
  waiting for transfers between devices  87.4 us (39%)
  between operations  13.7 us (6%)
  matrix products  9.46 us (4%)
  starting transfers between devices  8.88 us (4%)
  local copies, waits for them, and re-layouts  8.6 us (4%)
  other arithmetic  7.27 us (3%)
    reduce_scatter x1, waiting for transfers between devices, body(): lax.psum_scatter(partial_value.astype(jnp.bfloat16), 'tp', scatter_dimens...  38 us
    all_gather x1, blocking collectives, body(): lax.all_gather(key_rot, 'sp', axis=0, tiled=True)  32.6 us
    all_gather x1, blocking collectives, body(): lax.all_gather(value_proj, 'sp', axis=0, tiled=True)  30.7 us
    all_gather x1, waiting for transfers between devices, body(): lax.all_gather(received[None], 'tp', axis=0, tiled=True)  26.7 us
    all_to_all x1, blocking collectives, body(): lax.all_to_all(outgoing, 'sp', split_axis=0, concat_axis=0, tiled=True)  25.4 us
    all_to_all x1, waiting for transfers between devices, body(): lax.all_to_all(expert_out, 'sp', split_axis=0, concat_axis=0, tiled=True)  19.4 us
    all_to_all x1, starting transfers between devices, body(): lax.all_to_all(expert_out, 'sp', split_axis=0, concat_axis=0, tiled=True)  5.52 us
  transfers between devices with their start and end apart: 4, of which 4 were waited for; matrix products, arithmetic and copies ran while one was open for 1% of the time, Pallas kernels for 0%

commit v1 on v0

v1 whole, which is shorter than its diff:
```python
import functools

import jax
import jax.numpy as jnp
import numpy as np
from jax import lax
from jax.experimental import pallas as pl
from jax.experimental.pallas import tpu as pltpu
from jax.sharding import PartitionSpec as P

HEAD_DIM = 64
TOPK = 2
GRID_W = 64
TOK_DEV = 256
LANES = 128

eps = 1e-06
rope_base = 10000.0

BF = jnp.bfloat16
F32 = jnp.float32
MESH = pl.DeviceIdType.MESH


def rotary_table(tokens):
    positions = np.arange(tokens)
    freq_count = HEAD_DIM // 4
    inverse = (rope_base ** (-np.arange(freq_count, dtype=np.float32) / freq_count)).astype(np.float32)
    row_pos = (positions // GRID_W).astype(np.float32)
    col_pos = (positions % GRID_W).astype(np.float32)
    angles = np.concatenate([row_pos[:, None] * inverse, col_pos[:, None] * inverse], axis=-1)
    angles = angles.astype(np.float32)
    return np.concatenate([np.cos(angles), np.sin(angles)], axis=-1).astype(np.float32)


def lane_of(shape):
    return lax.broadcasted_iota(jnp.int32, shape, 1)


def prepare(x, gain, cos4, sin4):
    lane = lane_of(x.shape)
    low = lane < HEAD_DIM
    sq = x * x
    s_low = jnp.sum(jnp.where(low, sq, 0.0), axis=-1, keepdims=True) / HEAD_DIM
    s_high = jnp.sum(jnp.where(low, 0.0, sq), axis=-1, keepdims=True) / HEAD_DIM
    y = x * jnp.where(low, lax.rsqrt(s_low + eps), lax.rsqrt(s_high + eps)) * gain
    half = HEAD_DIM // 2
    first = (lane % HEAD_DIM) < half
    swapped = jnp.where(first, pltpu.roll(y, LANES - half, 1), pltpu.roll(y, half, 1))
    return y * cos4 + swapped * sin4


def kernel(
    n, cap, groups,
    resid_h, q_ref, k_ref, v_ref, qg_ref, kg_ref, ow_h, ng_ref, gw_h, uw_h, dw_h, ids_ref, rw_ref, tab_h,
    out_ref,
    resid, ow, gw, uw, dw, tab, kv, qx, mx, acc, att, attg, res_f, send, rows, hid, hidg, back, ret,
    loc, kv_ss, kv_rs, kf_ss, kf_rs, at_ss, at_rs, dw_ss, dw_rs, a_ss, a_rs, x_ss, x_rs,
    s_ss, s_rs, o_ss, o_rs, h_ss, h_rs, r_ss, r_rs,
):
    tok = q_ref.shape[0]
    tp = 4
    rown = tok // tp
    width = out_ref.shape[1]
    per = n // groups
    half_n = n // 2
    e = lax.axis_index("sp")
    j = lax.axis_index("tp")
    jx, jc = j // 2, j % 2
    xp = (1 - jx) * 2 + jc
    sib = jx * 2 + (1 - jc)
    a, b = e // 2, e % 2
    ypart = a * 2 + (1 - b)

    def rcopy(src, dst, ss, rs, s_id, t_id):
        return pltpu.make_async_remote_copy(
            src_ref=src, dst_ref=dst, send_sem=ss, recv_sem=rs,
            device_id=(s_id, t_id), device_id_type=MESH,
        )

    locals_ = [
        pltpu.make_async_copy(tab_h.at[pl.ds(e * tok, tok)], tab, loc.at[0]),
        pltpu.make_async_copy(dw_h.at[0], dw.at[j], loc.at[1]),
        pltpu.make_async_copy(ow_h, ow, loc.at[2]),
        pltpu.make_async_copy(resid_h, resid, loc.at[3]),
        pltpu.make_async_copy(gw_h.at[0], gw, loc.at[4]),
        pltpu.make_async_copy(uw_h.at[0], uw, loc.at[5]),
    ]
    for c in locals_:
        c.start()

    barrier = pltpu.get_barrier_semaphore()

    def greet(k, carry):
        pl.semaphore_signal(barrier, inc=1, device_id=(lax.rem(e + k, n), j), device_id_type=MESH)
        return carry

    lax.fori_loop(1, n, greet, 0)
    for k in range(1, tp):
        pl.semaphore_signal(barrier, inc=1, device_id=(e, lax.rem(j + k, tp)), device_id_type=MESH)

    locals_[0].wait()
    cs = tab[:, : HEAD_DIM // 2]
    sn = tab[:, HEAD_DIM // 2 :]
    cos4 = jnp.concatenate([cs, cs, cs, cs], axis=1)
    sin4 = jnp.concatenate([-sn, sn, -sn, sn], axis=1)
    k_in = k_ref[...].astype(F32)
    v_in = v_ref[...].astype(F32)
    low = lane_of((tok, LANES)) < HEAD_DIM
    kv_in = jnp.concatenate([k_in, v_in], axis=1)
    kgain = jnp.concatenate([kg_ref[...], kg_ref[...]], axis=1)
    kv[e] = jnp.where(low, prepare(kv_in, kgain, cos4, sin4), kv_in).astype(BF)
    pl.semaphore_wait(barrier, n - 1 + tp - 1)

    def kv_send(d):
        to = lax.rem(a + d, half_n) * 2 + b
        return rcopy(kv.at[e], kv.at[e], kv_ss.at[d], kv_rs.at[d], to, j)

    def kv_recv(d):
        src = lax.rem(a + half_n - d, half_n) * 2 + b
        return rcopy(kv.at[src], kv.at[src], kv_ss.at[d], kv_rs.at[d], e, j)

    def kf_send(d):
        src = lax.rem(a + half_n - d, half_n) * 2 + b
        return rcopy(kv.at[src], kv.at[src], kf_ss.at[d], kf_rs.at[d], ypart, j)

    def kf_recv(d):
        src = lax.rem(a + half_n - d, half_n) * 2 + (1 - b)
        return rcopy(kv.at[src], kv.at[src], kf_ss.at[d], kf_rs.at[d], ypart, j)

    def loop(lo, hi, fn):
        def step(i, carry):
            fn(i)
            return carry
        lax.fori_loop(lo, hi, step, 0)

    loop(1, half_n, lambda d: kv_send(d).start())
    kf_send(0).start()

    locals_[1].wait()
    dw_x = rcopy(dw.at[j], dw.at[j], dw_ss.at[0], dw_rs.at[0], e, xp)
    dw_s = rcopy(dw.at[j], dw.at[j], dw_ss.at[1], dw_rs.at[1], e, sib)
    dw_o = rcopy(dw.at[xp], dw.at[xp], dw_ss.at[2], dw_rs.at[2], e, sib)
    dw_x.start()
    dw_s.start()

    qgain = jnp.concatenate([qg_ref[0:1, :], qg_ref[1:2, :]], axis=1)
    q = prepare(q_ref[...].astype(F32), qgain, cos4, sin4) * (HEAD_DIM**-0.5)
    qx[0:tok] = jnp.where(low, q, 0.0).astype(BF)
    qx[tok : 2 * tok] = jnp.where(low, pltpu.roll(q, HEAD_DIM, 1), 0.0).astype(BF)
    mx[...] = jnp.full(mx.shape, -jnp.inf, F32)
    acc[...] = jnp.zeros(acc.shape, F32)

    def attend(d):
        @pl.when(d > 0)
        def _():
            kv_recv(d).wait_recv()
            kf_send(d).start()

        kf_recv(d).wait_recv()
        base = lax.rem(a + half_n - d, half_n) * 2
        keys = jnp.concatenate([kv[base], kv[base + 1]], axis=0)
        vals = jnp.where(lane_of(keys.shape) < HEAD_DIM, jnp.ones_like(keys), keys)
        for blk in range(4):
            rs = pl.ds(blk * (2 * tok // 4), 2 * tok // 4)
            sc = lax.dot_general(qx[rs], keys, (((1,), (1,)), ((), ())), preferred_element_type=F32)
            old = mx[rs]
            new = jnp.maximum(old, jnp.max(sc, axis=-1, keepdims=True))
            p = jnp.exp(sc - new[:, 0:1])
            mx[rs] = new
            acc[rs] = acc[rs] * jnp.exp(old - new) + jnp.dot(p.astype(BF), vals, preferred_element_type=F32)

    loop(0, half_n, attend)
    o = acc[...]
    o = o / pltpu.roll(o, HEAD_DIM, 1)
    att[...] = jnp.where(low, pltpu.roll(o[0:tok], HEAD_DIM, 1), o[tok : 2 * tok]).astype(BF)

    def at_copy(k):
        to = lax.rem(j + k, tp)
        return rcopy(att.at[pl.ds(to * rown, rown)], attg.at[j], at_ss.at[k], at_rs.at[k], e, to)

    def at_recv(k):
        src = lax.rem(j + tp - k, tp)
        return rcopy(att.at[pl.ds(0, rown)], attg.at[src], at_ss.at[k], at_rs.at[k], e, src)

    for k in range(1, tp):
        at_copy(k).start()
    attg[j] = att[pl.ds(j * rown, rown), :]

    slots = n * cap
    ids = ids_ref[pl.ds(j * rown, rown), :]
    rw = rw_ref[...]
    col = lax.broadcasted_iota(jnp.int32, (rown, slots), 1)
    off0 = col - ids[:, 0:1] * cap
    off1 = col - ids[:, 1:2] * cap
    in0 = (off0 >= 0) & (off0 < cap)
    in1 = (off1 >= 0) & (off1 < cap)
    member = jnp.where(in0 | in1, 1.0, 0.0)
    ti = lax.broadcasted_iota(jnp.int32, (rown, rown), 0)
    tj = lax.broadcasted_iota(jnp.int32, (rown, rown), 1)
    before = jnp.where(tj < ti, 1.0, 0.0)
    rank = jnp.dot(before.astype(BF), member.astype(BF), preferred_element_type=F32)
    offset = jnp.where(in0, off0, off1).astype(F32)
    hit = jnp.where(rank == offset, member, 0.0)
    weight = hit * jnp.where(in0, rw[:, 0:1], rw[:, 1:2])

    locals_[2].wait()
    locals_[3].wait()
    for k in range(1, tp):
        at_recv(k).wait_recv()
    joined = jnp.concatenate([attg[i] for i in range(tp)], axis=1)
    mixed = jnp.dot(joined, ow[...], preferred_element_type=F32)
    residual = (resid[...].astype(F32) + mixed).astype(BF).astype(F32)
    res_f[...] = residual
    scale = lax.rsqrt(jnp.mean(residual * residual, axis=-1, keepdims=True) + eps)
    normed = (residual * scale * ng_ref[...]).astype(BF)
    out_rows = lax.dot_general(
        hit.astype(BF), normed, (((0,), (0,)), ((), ())), preferred_element_type=F32
    )
    send[...] = out_rows.reshape(n, cap, width).astype(BF)

    def a_send(k):
        to = lax.rem(e + k, n)
        return rcopy(send.at[to], rows.at[j, k], a_ss.at[k], a_rs.at[k], to, j)

    def a_recv(k):
        return rcopy(send.at[0], rows.at[j, k], a_ss.at[k], a_rs.at[k], e, j)

    loop(1, n, lambda k: a_send(k).start())
    rows[j, 0] = send[e]
    dw_x_in = rcopy(dw.at[xp], dw.at[xp], dw_ss.at[0], dw_rs.at[0], e, xp)
    dw_x_in.wait_recv()
    dw_o.start()
    locals_[4].wait()
    locals_[5].wait()

    def part(t, g):
        return rows.at[t, pl.ds(g * per, per)]

    def x_send(g):
        return rcopy(part(j, g), part(j, g), x_ss.at[g], x_rs.at[g], e, xp)

    def x_recv(g):
        return rcopy(part(xp, g), part(xp, g), x_ss.at[g], x_rs.at[g], e, xp)

    def s_send(g):
        return rcopy(part(j, g), part(j, g), s_ss.at[g], s_rs.at[g], e, sib)

    def s_recv(g):
        return rcopy(part(sib, g), part(sib, g), s_ss.at[g], s_rs.at[g], e, sib)

    def o_send(g):
        return rcopy(part(xp, g), part(xp, g), o_ss.at[g], o_rs.at[g], e, sib)

    dg = (1 - jx) * 2 + (1 - jc)

    def o_recv(g):
        return rcopy(part(dg, g), part(dg, g), o_ss.at[g], o_rs.at[g], e, sib)

    def h_send(g, k):
        to = lax.rem(j + k, tp)
        return rcopy(hid.at[g, to], hidg.at[g, j], h_ss.at[g, k], h_rs.at[g, k], e, to)

    def h_recv(g, k):
        src = lax.rem(j + tp - k, tp)
        return rcopy(hid.at[g, 0], hidg.at[g, src], h_ss.at[g, k], h_rs.at[g, k], e, src)

    def r_send(k):
        to = lax.rem(e + n - k, n)
        return rcopy(back.at[k], ret.at[e], r_ss.at[k], r_rs.at[k], to, j)

    def r_recv(k):
        src = lax.rem(e + k, n)
        return rcopy(back.at[k], ret.at[src], r_ss.at[k], r_rs.at[k], e, j)

    m = per * cap

    def stage_a(g):
        def one(i):
            k = g * per + i

            @pl.when(k > 0)
            def _():
                a_recv(k).wait_recv()

        loop(0, per, one)
        x_send(g).start()
        s_send(g).start()

    def stage_c(g):
        x_recv(g).wait_recv()
        o_send(g).start()
        s_recv(g).wait_recv()
        o_recv(g).wait_recv()
        block = rows[:, pl.ds(g * per, per)].astype(F32).reshape(tp * m, width).astype(BF)
        gate = jnp.dot(block, gw[...], preferred_element_type=F32)
        upper = jnp.dot(block, uw[...], preferred_element_type=F32)
        hidden = gate / (1.0 + jnp.exp(-gate)) * upper
        hid[g] = hidden.reshape(tp, m, hidden.shape[1]).astype(BF)
        for k in range(1, tp):
            h_send(g, k).start()
        hidg[g, j] = hid[g, j]

    def stage_d(g):
        for k in range(1, tp):
            h_recv(g, k).wait_recv()

        @pl.when(g == 0)
        def _():
            rcopy(dw.at[sib], dw.at[sib], dw_ss.at[1], dw_rs.at[1], e, sib).wait_recv()
            rcopy(dw.at[dg], dw.at[dg], dw_ss.at[2], dw_rs.at[2], e, sib).wait_recv()

        joined_h = jnp.concatenate([hidg[g, i] for i in range(tp)], axis=1)
        cols = 512

        def column(ci):
            cd = pl.ds(pl.multiple_of(ci * cols, cols), cols)
            dfull = dw[:, :, cd].reshape(joined_h.shape[1], cols)
            y = jnp.dot(joined_h, dfull, preferred_element_type=F32)
            back[pl.ds(g * per, per), :, cd] = y.reshape(per, cap, cols).astype(BF)

        for ci in range(width // cols):
            column(ci)

        def one(i):
            k = g * per + i

            @pl.when(k > 0)
            def _():
                r_send(k).start()

        loop(0, per, one)

    def tick(t):
        @pl.when(t < groups)
        def _():
            stage_a(t)

        @pl.when(t >= 2)
        def _():
            stage_d(t - 2)

        @pl.when((t >= 1) & (t <= groups))
        def _():
            stage_c(t - 1)

    loop(0, groups + 2, tick)
    ret[e] = back[0]
    loop(1, n, lambda k: r_recv(k).wait_recv())
    w_hi = weight.astype(BF)
    w_lo = (weight - w_hi.astype(F32)).astype(BF)
    back_rows = ret[...].astype(F32).reshape(slots, width).astype(BF)
    total = jnp.dot(w_hi, back_rows, preferred_element_type=F32)
    total += jnp.dot(w_lo, back_rows, preferred_element_type=F32)
    out_ref[...] = (res_f[...] + total).astype(BF)

    def drain(k):
        a_send(k).wait_send()
        r_send(k).wait_send()

    loop(1, n, drain)
    loop(1, half_n, lambda d: kv_send(d).wait_send())
    loop(0, half_n, lambda d: kf_send(d).wait_send())
    for k in range(1, tp):
        at_copy(k).wait_send()
    dw_x.wait_send()
    dw_s.wait_send()
    dw_o.wait_send()

    def drain_g(g):
        x_send(g).wait_send()
        s_send(g).wait_send()
        o_send(g).wait_send()
        for k in range(1, tp):
            h_send(g, k).wait_send()

    loop(0, groups, drain_g)


def body(resid_in, query_proj, key_proj, value_proj, query_gain, key_gain, out_weight, norm_gain,
         gate_weight, up_weight, down_weight, expert_ids, route_weight):
    n = lax.axis_size("sp")
    tp = lax.axis_size("tp")
    tok = query_proj.shape[0]
    rown = tok // tp
    width = resid_in.shape[1]
    ff = gate_weight.shape[2]
    need = max(2, 3 * TOPK * TOK_DEV // (2 * tp * n))
    cap = -(-need // 8) * 8
    groups = 4
    per = n // groups
    table = jnp.asarray(rotary_table(n * tok))
    vm = pl.BlockSpec(memory_space=pltpu.VMEM)
    hb = pl.BlockSpec(memory_space=pl.ANY)
    dma = pltpu.SemaphoreType.DMA
    V = pltpu.VMEM
    scratch = [
        V((rown, width), BF),
        V(out_weight.shape, BF),
        V((width, ff), BF),
        V((width, ff), BF),
        V((tp, ff, width), BF),
        V((tok, HEAD_DIM), F32),
        V((n, tok, LANES), BF),
        V((2 * tok, LANES), BF),
        V((2 * tok, LANES), F32),
        V((2 * tok, LANES), F32),
        V((tok, LANES), BF),
        V((tp, rown, LANES), BF),
        V((rown, width), F32),
        V((n, cap, width), BF),
        V((tp, n, cap, width), BF),
        V((groups, tp, per * cap, ff), BF),
        V((groups, tp, per * cap, ff), BF),
        V((n, cap, width), BF),
        V((n, cap, width), BF),
        dma((6,)),
        dma((n // 2,)), dma((n // 2,)), dma((n // 2,)), dma((n // 2,)),
        dma((tp,)), dma((tp,)), dma((3,)), dma((3,)),
        dma((n,)), dma((n,)),
        dma((groups,)), dma((groups,)), dma((groups,)), dma((groups,)), dma((groups,)), dma((groups,)),
        dma((groups, tp)), dma((groups, tp)),
        dma((n,)), dma((n,)),
    ]
    return pl.pallas_call(
        functools.partial(kernel, n, cap, groups),
        out_shape=jax.ShapeDtypeStruct((rown, width), BF),
        in_specs=[hb, vm, vm, vm, vm, vm, hb, vm, hb, hb, hb, vm, vm, hb],
        out_specs=vm,
        scratch_shapes=scratch,
        compiler_params=pltpu.CompilerParams(
            collective_id=0, has_side_effects=True, vmem_limit_bytes=60 * 1024 * 1024
        ),
    )(resid_in, query_proj, key_proj, value_proj, query_gain, key_gain, out_weight,
      norm_gain.reshape(1, width), gate_weight, up_weight, down_weight, expert_ids, route_weight, table)


def solution(mesh):
    placed = (
        P(("sp", "tp"), None),
        P("sp", "tp"),
        P("sp", "tp"),
        P("sp", "tp"),
        P("tp", None),
        P("tp", None),
        P(),
        P(),
        P("sp", None, "tp"),
        P("sp", None, "tp"),
        P("sp", "tp", None),
        P("sp", None),
        P(("sp", "tp"), None),
    )
    return jax.shard_map(
        body, mesh=mesh, in_specs=placed, out_specs=P(("sp", "tp"), None), check_vma=False
    )
```

time: 225 us -> 90 us (0.40)
  blocking collectives: 88.7 us -> 0 us
  waiting for transfers between devices: 87.4 us -> 0 us
  Pallas kernels: 0 us -> 82.2 us
  between operations: 13.7 us -> 0.01 us
  matrix products: 9.46 us -> 0 us
  starting transfers between devices: 8.88 us -> 0 us
  other arithmetic: 7.27 us -> 0 us
    pallas_call x0 -> x1, Pallas kernels: none -> 82.2 us  [body(): pl.pallas_call(functools.partial(kernel, n, cap, groups), out_shape=jax.S...]
    all_gather x2 -> x0, blocking collectives: 63.3 us -> none  [the longest x1 32.6 us: body(): lax.all_gather(key_rot, 'sp', axis=0, tiled=True)]
    reduce_scatter x1 -> x0, waiting for transfers between devices: 38 us -> none  [body(): lax.psum_scatter(partial_value.astype(jnp.bfloat16), 'tp', scatter_dimens...]
    all_gather x1 -> x0, waiting for transfers between devices: 26.7 us -> none  [body(): lax.all_gather(received[None], 'tp', axis=0, tiled=True)]
    all_to_all x1 -> x0, blocking collectives: 25.4 us -> none  [body(): lax.all_to_all(outgoing, 'sp', split_axis=0, concat_axis=0, tiled=True)]
    all_to_all x2 -> x0, waiting for transfers between devices: 22.6 us -> none  [the longest x1 19.4 us: body(): lax.all_to_all(expert_out, 'sp', split_axis=0, concat_axis=0, tiled=True)]
    dot_general x7 -> x0, matrix products: 9.46 us -> none  [the longest x1 3.31 us: expert_ffn(): gate = jnp.dot(flat_rows, gate_local, preferred_element_type=jnp.float32)]
    all_to_all x2 -> x0, starting transfers between devices: 8.8 us -> none  [the longest x1 5.52 us: body(): lax.all_to_all(expert_out, 'sp', split_axis=0, concat_axis=0, tiled=True)]
  transfers between devices with their start and end apart: 4 -> 0, of which waited for: 4 -> 0; matrix products, arithmetic and copies ran while one was open for 1% -> 0% of each run, Pallas kernels for 0% -> 0%
where the time goes in v1:
time: 90 us; the launch traced here: 89.7 us
  Pallas kernels  82.2 us (91%)
  local copies, waits for them, and re-layouts  7.48 us (8%)
    pallas_call x1, Pallas kernels, body(): pl.pallas_call(functools.partial(kernel, n, cap, groups), out_shape=jax.S...  82.2 us
    unnamed x5, local copies, waits for them, and re-layouts  7.48 us

profile of v1, /device:TPU:0, one launch (start us, length us, event | category | flops | bytes accessed | tf_op | source)
XLA Modules:
  0.0 89.7 jit_solution(5160163669815280990)
XLA Ops:
  0.0 1.4 %copy.18.rw_ref = f32[64,2]{1,0:T(8,128)} copy(f32[64,2]{0,1:T(2,128)} %param.26) | data formatting | bytes 1024 | tf_op args[12]
  1.4 1.5 %copy.15.k_ref = bf16[256,64]{1,0:T(8,128)(2,1)} copy(bf16[256,64]{0,1:T(8,128)(2,1)} %param.16) | data formatting | bytes 65536 | tf_op args[2]
  2.8 1.5 %copy.16.v_ref = bf16[256,64]{1,0:T(8,128)(2,1)} copy(bf16[256,64]{0,1:T(8,128)(2,1)} %param.17) | data formatting | bytes 65536 | tf_op args[3]
  4.3 1.5 %copy.17.ids_ref = s32[256,2]{1,0:T(8,128)} copy(s32[256,2]{0,1:T(2,128)} %param.25) | data formatting | bytes 4096 | tf_op args[11]
  5.8 82.2 %shard_map.136 = bf16[64,2048]{1,0:T(8,128)(2,1)} custom-call(bf16[64,2048]{1,0:T(8,128)(2,1)} %resid_h.1, bf16[256,128]{1,0:T(8,128)(2,1)} %q_ref.1, bf16[256,64]{1,0:T(8,128)(2,1)} %copy.15.k_ref, bf16[256,64]{1,0:T(8,128)(2,1)} %copy.16.v_ref, f32[2,64]{1,0:T(2,128)} %qg_ref.1, f32[1,64]{1,0:T(1,128)} %kg_ref.1, bf16[512,2048]{1,0:T(8,128)(2,1)} %ow_h.1, ...), custom_call_target="tpu_custom_call" | custom-call | tf_op jit(solution)/shard_map/pallas_call | solution.py:425
  88.0 1.7 %copy.20 = bf16[64,2048]{1,0:T(8,128)(2,1)} copy(bf16[64,2048]{1,0:T(8,128)(2,1)} %shard_map.136) | data formatting | bytes 524288

commit v2 on v1

--- a/solution.py
+++ b/solution.py
@@ -54,7 +54,7 @@
     n, cap, groups,
     resid_h, q_ref, k_ref, v_ref, qg_ref, kg_ref, ow_h, ng_ref, gw_h, uw_h, dw_h, ids_ref, rw_ref, tab_h,
     out_ref,
-    resid, ow, gw, uw, dw, tab, kv, qx, mx, acc, att, attg, res_f, send, rows, hid, hidg, back, ret,
+    resid, ow, gw, uw, dw, tab, kv, qx, mx, acc, att, attg, res_f, send, rows, hid, hidg, back, ret, ids_t,
     loc, kv_ss, kv_rs, kf_ss, kf_rs, at_ss, at_rs, dw_ss, dw_rs, a_ss, a_rs, x_ss, x_rs,
     s_ss, s_rs, o_ss, o_rs, h_ss, h_rs, r_ss, r_rs,
 ):
@@ -104,10 +104,8 @@
     sn = tab[:, HEAD_DIM // 2 :]
     cos4 = jnp.concatenate([cs, cs, cs, cs], axis=1)
     sin4 = jnp.concatenate([-sn, sn, -sn, sn], axis=1)
-    k_in = k_ref[...].astype(F32)
-    v_in = v_ref[...].astype(F32)
     low = lane_of((tok, LANES)) < HEAD_DIM
-    kv_in = jnp.concatenate([k_in, v_in], axis=1)
+    kv_in = jnp.concatenate([k_ref[...].astype(F32), v_ref[...].astype(F32)], axis=0).T
     kgain = jnp.concatenate([kg_ref[...], kg_ref[...]], axis=1)
     kv[e] = jnp.where(low, prepare(kv_in, kgain, cos4, sin4), kv_in).astype(BF)
     pl.semaphore_wait(barrier, n - 1 + tp - 1)
@@ -138,10 +136,17 @@
     kf_send(0).start()
 
     locals_[1].wait()
-    dw_x = rcopy(dw.at[j], dw.at[j], dw_ss.at[0], dw_rs.at[0], e, xp)
+    ff = dw.shape[1]
+    early = 3 * ff // 4
+
+    def dw_x(part_id, owner):
+        rows_of = pl.ds(0, early) if part_id == 0 else pl.ds(early, ff - early)
+        sem = 3 * part_id
+        return rcopy(dw.at[owner, rows_of], dw.at[owner, rows_of], dw_ss.at[sem], dw_rs.at[sem], e, xp)
+
     dw_s = rcopy(dw.at[j], dw.at[j], dw_ss.at[1], dw_rs.at[1], e, sib)
     dw_o = rcopy(dw.at[xp], dw.at[xp], dw_ss.at[2], dw_rs.at[2], e, sib)
-    dw_x.start()
+    dw_x(0, j).start()
     dw_s.start()
 
     qgain = jnp.concatenate([qg_ref[0:1, :], qg_ref[1:2, :]], axis=1)
@@ -185,11 +190,14 @@
 
     for k in range(1, tp):
         at_copy(k).start()
+    dw_x(1, j).start()
     attg[j] = att[pl.ds(j * rown, rown), :]
 
     slots = n * cap
-    ids = ids_ref[pl.ds(j * rown, rown), :]
-    rw = rw_ref[...]
+    ids_f = jnp.concatenate([ids_ref[...].astype(F32), jnp.zeros((6, tok), F32)], axis=0)
+    ids_t[...] = ids_f.T
+    ids = ids_t[pl.ds(j * rown, rown), :].astype(jnp.int32)
+    rw = jnp.concatenate([rw_ref[...], jnp.zeros((6, rown), F32)], axis=0).T
     col = lax.broadcasted_iota(jnp.int32, (rown, slots), 1)
     off0 = col - ids[:, 0:1] * cap
     off1 = col - ids[:, 1:2] * cap
@@ -228,9 +236,6 @@
 
     loop(1, n, lambda k: a_send(k).start())
     rows[j, 0] = send[e]
-    dw_x_in = rcopy(dw.at[xp], dw.at[xp], dw_ss.at[0], dw_rs.at[0], e, xp)
-    dw_x_in.wait_recv()
-    dw_o.start()
     locals_[4].wait()
     locals_[5].wait()
 
@@ -290,6 +295,13 @@
     def stage_c(g):
         x_recv(g).wait_recv()
         o_send(g).start()
+
+        @pl.when(g == 0)
+        def _():
+            dw_x(0, xp).wait_recv()
+            dw_x(1, xp).wait_recv()
+            dw_o.start()
+
         s_recv(g).wait_recv()
         o_recv(g).wait_recv()
         block = rows[:, pl.ds(g * per, per)].astype(F32).reshape(tp * m, width).astype(BF)
@@ -363,7 +375,8 @@
     loop(0, half_n, lambda d: kf_send(d).wait_send())
     for k in range(1, tp):
         at_copy(k).wait_send()
-    dw_x.wait_send()
+    dw_x(0, j).wait_send()
+    dw_x(1, j).wait_send()
     dw_s.wait_send()
     dw_o.wait_send()
 
@@ -387,7 +400,7 @@
     ff = gate_weight.shape[2]
     need = max(2, 3 * TOPK * TOK_DEV // (2 * tp * n))
     cap = -(-need // 8) * 8
-    groups = 4
+    groups = min(4, n)
     per = n // groups
     table = jnp.asarray(rotary_table(n * tok))
     vm = pl.BlockSpec(memory_space=pltpu.VMEM)
@@ -414,15 +427,16 @@
         V((groups, tp, per * cap, ff), BF),
         V((n, cap, width), BF),
         V((n, cap, width), BF),
+        V((tok, 8), F32),
         dma((6,)),
         dma((n // 2,)), dma((n // 2,)), dma((n // 2,)), dma((n // 2,)),
-        dma((tp,)), dma((tp,)), dma((3,)), dma((3,)),
+        dma((tp,)), dma((tp,)), dma((4,)), dma((4,)),
         dma((n,)), dma((n,)),
         dma((groups,)), dma((groups,)), dma((groups,)), dma((groups,)), dma((groups,)), dma((groups,)),
         dma((groups, tp)), dma((groups, tp)),
         dma((n,)), dma((n,)),
     ]
-    return pl.pallas_call(
+    out = pl.pallas_call(
         functools.partial(kernel, n, cap, groups),
         out_shape=jax.ShapeDtypeStruct((rown, width), BF),
         in_specs=[hb, vm, vm, vm, vm, vm, hb, vm, hb, hb, hb, vm, vm, hb],
@@ -431,8 +445,9 @@
         compiler_params=pltpu.CompilerParams(
             collective_id=0, has_side_effects=True, vmem_limit_bytes=60 * 1024 * 1024
         ),
-    )(resid_in, query_proj, key_proj, value_proj, query_gain, key_gain, out_weight,
-      norm_gain.reshape(1, width), gate_weight, up_weight, down_weight, expert_ids, route_weight, table)
+    )(resid_in, query_proj, key_proj.T, value_proj.T, query_gain, key_gain, out_weight,
+      norm_gain.reshape(1, width), gate_weight, up_weight, down_weight, expert_ids.T, route_weight.T, table)
+    return out
 
 
 def solution(mesh):

time: 90 us -> 81.1 us (0.901)
  local copies, waits for them, and re-layouts: 7.48 us -> 1.67 us
  Pallas kernels: 82.2 us -> 79.2 us
    unnamed x5 -> x1, local copies, waits for them, and re-layouts: 7.48 us -> 1.67 us
    pallas_call x1, Pallas kernels: 82.2 us -> 79.2 us  [body(): pl.pallas_call(functools.partial(kernel, n, cap, groups), out_shape=jax.S...]
where the time goes in v2:
time: 81.1 us; the launch traced here: 80.9 us
  Pallas kernels  79.2 us (98%)
  local copies, waits for them, and re-layouts  1.67 us (2%)
    pallas_call x1, Pallas kernels, body(): pl.pallas_call(functools.partial(kernel, n, cap, groups), out_shape=jax.S...  79.2 us
    unnamed x1, local copies, waits for them, and re-layouts  1.67 us

profile of v2, /device:TPU:0, one launch (start us, length us, event | category | flops | bytes accessed | tf_op | source)
XLA Modules:
  0.0 80.9 jit_solution(16732021784491322856)
XLA Ops:
  0.0 79.2 %shard_map.136 = bf16[64,2048]{1,0:T(8,128)(2,1)} custom-call(bf16[64,2048]{1,0:T(8,128)(2,1)} %resid_h.1, bf16[256,128]{1,0:T(8,128)(2,1)} %q_ref.1, bf16[64,256]{1,0:T(8,128)(2,1)} %bitcast.5, bf16[64,256]{1,0:T(8,128)(2,1)} %bitcast.6, f32[2,64]{1,0:T(2,128)} %qg_ref.1, f32[1,64]{1,0:T(1,128)} %kg_ref.1, bf16[512,2048]{1,0:T(8,128)(2,1)} %ow_h.1, ...), custom_call_target="tpu_custom_call" | custom-call | tf_op jit(solution)/shard_map/pallas_call | solution.py:439
  79.3 1.7 %copy.16 = bf16[64,2048]{1,0:T(8,128)(2,1)} copy(bf16[64,2048]{1,0:T(8,128)(2,1)} %shard_map.136) | data formatting | bytes 524288

commit v3 on v2

--- a/solution.py
+++ b/solution.py
@@ -108,53 +108,53 @@
     kv_in = jnp.concatenate([k_ref[...].astype(F32), v_ref[...].astype(F32)], axis=0).T
     kgain = jnp.concatenate([kg_ref[...], kg_ref[...]], axis=1)
     kv[e] = jnp.where(low, prepare(kv_in, kgain, cos4, sin4), kv_in).astype(BF)
-    pl.semaphore_wait(barrier, n - 1 + tp - 1)
-
-    def kv_send(d):
-        to = lax.rem(a + d, half_n) * 2 + b
-        return rcopy(kv.at[e], kv.at[e], kv_ss.at[d], kv_rs.at[d], to, j)
-
-    def kv_recv(d):
-        src = lax.rem(a + half_n - d, half_n) * 2 + b
-        return rcopy(kv.at[src], kv.at[src], kv_ss.at[d], kv_rs.at[d], e, j)
-
-    def kf_send(d):
-        src = lax.rem(a + half_n - d, half_n) * 2 + b
-        return rcopy(kv.at[src], kv.at[src], kf_ss.at[d], kf_rs.at[d], ypart, j)
-
-    def kf_recv(d):
-        src = lax.rem(a + half_n - d, half_n) * 2 + (1 - b)
-        return rcopy(kv.at[src], kv.at[src], kf_ss.at[d], kf_rs.at[d], ypart, j)
-
-    def loop(lo, hi, fn):
-        def step(i, carry):
-            fn(i)
-            return carry
-        lax.fori_loop(lo, hi, step, 0)
-
-    loop(1, half_n, lambda d: kv_send(d).start())
-    kf_send(0).start()
-
-    locals_[1].wait()
-    ff = dw.shape[1]
-    early = 3 * ff // 4
-
-    def dw_x(part_id, owner):
-        rows_of = pl.ds(0, early) if part_id == 0 else pl.ds(early, ff - early)
-        sem = 3 * part_id
-        return rcopy(dw.at[owner, rows_of], dw.at[owner, rows_of], dw_ss.at[sem], dw_rs.at[sem], e, xp)
-
-    dw_s = rcopy(dw.at[j], dw.at[j], dw_ss.at[1], dw_rs.at[1], e, sib)
-    dw_o = rcopy(dw.at[xp], dw.at[xp], dw_ss.at[2], dw_rs.at[2], e, sib)
-    dw_x(0, j).start()
-    dw_s.start()
-
     qgain = jnp.concatenate([qg_ref[0:1, :], qg_ref[1:2, :]], axis=1)
     q = prepare(q_ref[...].astype(F32), qgain, cos4, sin4) * (HEAD_DIM**-0.5)
     qx[0:tok] = jnp.where(low, q, 0.0).astype(BF)
     qx[tok : 2 * tok] = jnp.where(low, pltpu.roll(q, HEAD_DIM, 1), 0.0).astype(BF)
     mx[...] = jnp.full(mx.shape, -jnp.inf, F32)
     acc[...] = jnp.zeros(acc.shape, F32)
+
+    pl.semaphore_wait(barrier, n - 1 + tp - 1)
+
+    def kv_send(d):
+        to = lax.rem(a + d, half_n) * 2 + b
+        return rcopy(kv.at[e], kv.at[e], kv_ss.at[d], kv_rs.at[d], to, j)
+
+    def kv_recv(d):
+        src = lax.rem(a + half_n - d, half_n) * 2 + b
+        return rcopy(kv.at[src], kv.at[src], kv_ss.at[d], kv_rs.at[d], e, j)
+
+    def kf_send(d):
+        src = lax.rem(a + half_n - d, half_n) * 2 + b
+        return rcopy(kv.at[src], kv.at[src], kf_ss.at[d], kf_rs.at[d], ypart, j)
+
+    def kf_recv(d):
+        src = lax.rem(a + half_n - d, half_n) * 2 + (1 - b)
+        return rcopy(kv.at[src], kv.at[src], kf_ss.at[d], kf_rs.at[d], ypart, j)
+
+    def loop(lo, hi, fn):
+        def step(i, carry):
+            fn(i)
+            return carry
+        lax.fori_loop(lo, hi, step, 0)
+
+    loop(1, half_n, lambda d: kv_send(d).start())
+    kf_send(0).start()
+
+    locals_[1].wait()
+    ff = dw.shape[1]
+    early = 3 * ff // 4
+
+    def dw_x(part_id, owner):
+        rows_of = pl.ds(0, early) if part_id == 0 else pl.ds(early, ff - early)
+        sem = 3 * part_id
+        return rcopy(dw.at[owner, rows_of], dw.at[owner, rows_of], dw_ss.at[sem], dw_rs.at[sem], e, xp)
+
+    dw_s = rcopy(dw.at[j], dw.at[j], dw_ss.at[1], dw_rs.at[1], e, sib)
+    dw_o = rcopy(dw.at[xp], dw.at[xp], dw_ss.at[2], dw_rs.at[2], e, sib)
+    dw_x(0, j).start()
+    dw_s.start()
 
     def attend(d):
         @pl.when(d > 0)
@@ -174,24 +174,6 @@
             p = jnp.exp(sc - new[:, 0:1])
             mx[rs] = new
             acc[rs] = acc[rs] * jnp.exp(old - new) + jnp.dot(p.astype(BF), vals, preferred_element_type=F32)
-
-    loop(0, half_n, attend)
-    o = acc[...]
-    o = o / pltpu.roll(o, HEAD_DIM, 1)
-    att[...] = jnp.where(low, pltpu.roll(o[0:tok], HEAD_DIM, 1), o[tok : 2 * tok]).astype(BF)
-
-    def at_copy(k):
-        to = lax.rem(j + k, tp)
-        return rcopy(att.at[pl.ds(to * rown, rown)], attg.at[j], at_ss.at[k], at_rs.at[k], e, to)
-
-    def at_recv(k):
-        src = lax.rem(j + tp - k, tp)
-        return rcopy(att.at[pl.ds(0, rown)], attg.at[src], at_ss.at[k], at_rs.at[k], e, src)
-
-    for k in range(1, tp):
-        at_copy(k).start()
-    dw_x(1, j).start()
-    attg[j] = att[pl.ds(j * rown, rown), :]
 
     slots = n * cap
     ids_f = jnp.concatenate([ids_ref[...].astype(F32), jnp.zeros((6, tok), F32)], axis=0)
@@ -212,6 +194,24 @@
     hit = jnp.where(rank == offset, member, 0.0)
     weight = hit * jnp.where(in0, rw[:, 0:1], rw[:, 1:2])
 
+    loop(0, half_n, attend)
+    o = acc[...]
+    o = o / pltpu.roll(o, HEAD_DIM, 1)
+    att[...] = jnp.where(low, pltpu.roll(o[0:tok], HEAD_DIM, 1), o[tok : 2 * tok]).astype(BF)
+
+    def at_copy(k):
+        to = lax.rem(j + k, tp)
+        return rcopy(att.at[pl.ds(to * rown, rown)], attg.at[j], at_ss.at[k], at_rs.at[k], e, to)
+
+    def at_recv(k):
+        src = lax.rem(j + tp - k, tp)
+        return rcopy(att.at[pl.ds(0, rown)], attg.at[src], at_ss.at[k], at_rs.at[k], e, src)
+
+    for k in range(1, tp):
+        at_copy(k).start()
+    dw_x(1, j).start()
+    attg[j] = att[pl.ds(j * rown, rown), :]
+
     locals_[2].wait()
     locals_[3].wait()
     for k in range(1, tp):
@@ -227,8 +227,21 @@
     )
     send[...] = out_rows.reshape(n, cap, width).astype(BF)
 
+    def split(i):
+        p = i // 2
+        q = ((p + half_n - 1) // half_n) * (1 + p % (half_n - 1))
+        return q // 2, q % 2, i % 2
+
+    def target(i):
+        k0, k1, kb = split(i)
+        return ((a // 2 + k0) % (half_n // 2)) * 4 + ((a % 2 + k1) % 2) * 2 + (b + kb) % 2
+
+    def source(i):
+        k0, k1, kb = split(i)
+        return ((a // 2 + half_n // 2 - k0) % (half_n // 2)) * 4 + ((a % 2 + k1) % 2) * 2 + (b + kb) % 2
+
     def a_send(k):
-        to = lax.rem(e + k, n)
+        to = target(k)
         return rcopy(send.at[to], rows.at[j, k], a_ss.at[k], a_rs.at[k], to, j)
 
     def a_recv(k):
@@ -271,11 +284,11 @@
         return rcopy(hid.at[g, 0], hidg.at[g, src], h_ss.at[g, k], h_rs.at[g, k], e, src)
 
     def r_send(k):
-        to = lax.rem(e + n - k, n)
+        to = source(k)
         return rcopy(back.at[k], ret.at[e], r_ss.at[k], r_rs.at[k], to, j)
 
     def r_recv(k):
-        src = lax.rem(e + k, n)
+        src = target(k)
         return rcopy(back.at[k], ret.at[src], r_ss.at[k], r_rs.at[k], e, j)
 
     m = per * cap

time: 81.1 us -> 80.5 us (level)
  no operation moved by 1% of the time
where the time goes in v3:
time: 80.5 us; the launch traced here: 80.3 us
  Pallas kernels  78.7 us (98%)
  local copies, waits for them, and re-layouts  1.67 us (2%)
    pallas_call x1, Pallas kernels, body(): pl.pallas_call(functools.partial(kernel, n, cap, groups), out_shape=jax.S...  78.7 us
    unnamed x1, local copies, waits for them, and re-layouts  1.67 us

profile of v3, /device:TPU:0, one launch (start us, length us, event | category | flops | bytes accessed | tf_op | source)
XLA Modules:
  0.0 80.3 jit_solution(16466775123551591872)
XLA Ops:
  0.0 78.7 %shard_map.136 = bf16[64,2048]{1,0:T(8,128)(2,1)} custom-call(bf16[64,2048]{1,0:T(8,128)(2,1)} %resid_h.1, bf16[256,128]{1,0:T(8,128)(2,1)} %q_ref.1, bf16[64,256]{1,0:T(8,128)(2,1)} %bitcast.5, bf16[64,256]{1,0:T(8,128)(2,1)} %bitcast.6, f32[2,64]{1,0:T(2,128)} %qg_ref.1, f32[1,64]{1,0:T(1,128)} %kg_ref.1, bf16[512,2048]{1,0:T(8,128)(2,1)} %ow_h.1, ...), custom_call_target="tpu_custom_call" | custom-call | tf_op jit(solution)/shard_map/pallas_call | solution.py:452
  78.7 1.7 %copy.16 = bf16[64,2048]{1,0:T(8,128)(2,1)} copy(bf16[64,2048]{1,0:T(8,128)(2,1)} %shard_map.136) | data formatting | bytes 524288
